TPU v7x, 256 devices: a whole 4x4x8 slice. The times are simulated.
256 devices in a mesh: ep: 64 (over z, y, core), tp: 4 (over x).
Axes of the slice: x: 4, y: 4, z: 8, core: 2. Of those that a mesh axis runs over, the one named last changes fastest.
Arguments:
- mixer_input: bfloat16 [32768, 2048], P('ep'), may hold values from -6 to 6
- mixer_gain: bfloat16 [2048], replicated, may hold values from 0.099609375 to 1.8984375
- pool_in: bfloat16 [2048, 1024], P(None, 'tp'), may hold values from -0.125 to 0.125
- pool_map: bfloat16 [4, 256, 256], P('tp'), may hold values from -0.375 to 0.375
- pool_scale: bfloat16 [1024], P('tp'), may hold values from 0.099609375 to 1.8984375
- pool_out: bfloat16 [1024, 2048], P('tp'), may hold values from -0.1875 to 0.1875
- expert_input: bfloat16 [24576, 2048], P('ep'), may hold values from -6 to 6
- expert_gain: bfloat16 [2048], replicated, may hold values from 0.099609375 to 1.8984375
- group_router: bfloat16 [2048, 4], replicated, may hold values from -0.125 to 0.125
- expert_router: bfloat16 [2048, 64], replicated, may hold values from -0.125 to 0.125
- routes: int32 [24576, 2], P('ep'), may hold values from 0 to 63, all different within a row; in each aligned block of 96 rows (0 to 95, 96 to 191, ...) at most 6 rows name the same one
- gate_weight: bfloat16 [64, 2048, 1024], P('ep', None, 'tp'), may hold values from -0.125 to 0.125
- up_weight: bfloat16 [64, 2048, 1024], P('ep', None, 'tp'), may hold values from -0.125 to 0.125
- down_weight: bfloat16 [64, 1024, 2048], P('ep', 'tp'), may hold values from -0.1875 to 0.1875
Outputs:
- mixer_output: bfloat16 [32768, 2048], P(('ep', 'tp'))
- expert_output: bfloat16 [24576, 2048], P(('ep', 'tp'))
Inputs may be any that keep to these rules, and one draw needn't show every extreme that they name: `routes`: each row names two different experts. In each aligned block of 96 rows no expert is named more than 6 times, a bound that some block reaches.
All inputs are finite; a program needn't handle non-finite values.
Results may differ from a plain program's by a relative error of at most 0.01.
Values may be sent and summed in bfloat16 or wider, within the bound.
No kernel may reach another device: no remote copies, remote signals or barrier semaphores. Data moves between devices by JAX's collectives and lax.ppermute only.
A program may use at most 64 MiB of HBM per device.

v0:
```python
import jax
import jax.numpy as jnp
from jax import lax
from jax.sharding import PartitionSpec as P

RIM = 15
EPS = 1e-06


def passed_along(value, axis, steps):
    count = lax.axis_size(axis)
    leading, last = (max(0, -steps), min(count, count - steps))
    return lax.ppermute(value, axis, [(source, source + steps) for source in range(leading, last)])


def norm_rows(values, gain):
    floats = values.astype(jnp.float32)
    scale = lax.rsqrt(jnp.mean(floats * floats, axis=-1, keepdims=True) + EPS)
    return (floats * scale * gain.astype(jnp.float32)).astype(jnp.bfloat16)


def route_weights(rows, group_router, expert_router, route_rows):
    group_logits = jnp.dot(rows, group_router, preferred_element_type=jnp.float32)
    expert_logits = jnp.dot(rows, expert_router, preferred_element_type=jnp.float32)
    groups = group_logits.shape[1]
    experts = expert_logits.shape[1]
    member = (
        jnp.arange(experts, dtype=jnp.int32)[:, None] // (experts // groups)
        == jnp.arange(groups, dtype=jnp.int32)[None, :]
    ).astype(jnp.float32)
    group_exp = jnp.exp(group_logits)
    group_prob = group_exp / jnp.sum(group_exp, axis=1, keepdims=True)
    expert_exp = jnp.exp(expert_logits)
    within = jnp.dot(expert_exp, member, precision=lax.Precision.HIGHEST)
    prob = expert_exp * jnp.dot(group_prob / within, member.T, precision=lax.Precision.HIGHEST)
    chosen = (route_rows[:, :, None] == jnp.arange(experts, dtype=jnp.int32)[None, None, :]).astype(
        jnp.float32
    )
    picked = jnp.sum(chosen * prob[:, None, :], axis=2)
    return picked / jnp.sum(picked, axis=1, keepdims=True)


def mixer_half(mixer_input, mixer_gain, pool_in, pool_map, pool_scale, pool_out):
    normed = norm_rows(mixer_input, mixer_gain)
    pooled_in = jnp.dot(normed, pool_in, preferred_element_type=jnp.float32).astype(jnp.bfloat16)
    local_rows = pooled_in.shape[0]
    groups_here = pool_map.shape[0]
    channels = pool_map.shape[1]
    border = passed_along(pooled_in[local_rows - RIM :], "ep", 1)
    padded = jnp.concatenate([border, pooled_in], axis=0).astype(jnp.float32)
    padded = padded.reshape(local_rows + RIM, groups_here, channels)
    leading = lax.axis_index("tp") * groups_here
    windows = jnp.left_shift(jnp.int32(2), leading + jnp.arange(groups_here, dtype=jnp.int32))
    window_sum = jnp.zeros((local_rows, groups_here, channels), jnp.float32)
    for offset in range(RIM + 1):
        active = (offset < windows).astype(jnp.float32)
        window_sum = (
            window_sum + padded[RIM - offset : RIM - offset + local_rows] * active[None, :, None]
        )
    position = lax.axis_index("ep") * local_rows + jnp.arange(local_rows, dtype=jnp.int32)
    counts_here = jnp.minimum(position[:, None] + 1, windows[None, :]).astype(jnp.float32)
    pooled = (window_sum / counts_here[:, :, None] - padded[RIM:]).astype(jnp.bfloat16)
    mapped = jnp.einsum("tgc,gce->tge", pooled, pool_map, preferred_element_type=jnp.float32)
    mixed_rows = (
        mapped.reshape(local_rows, groups_here * channels) * pool_scale.astype(jnp.float32)
    ).astype(jnp.bfloat16)
    return lax.psum_scatter(
        jnp.dot(mixed_rows, pool_out, preferred_element_type=jnp.float32).astype(jnp.bfloat16),
        "tp",
        scatter_dimension=0,
        tiled=True,
    )


def slot_positions(route_rows, blocks, experts):
    flat = route_rows.reshape(blocks, -1)
    onehot = (flat[:, :, None] == jnp.arange(experts, dtype=jnp.int32)[None, None, :]).astype(
        jnp.int32
    )
    before = jnp.cumsum(onehot, axis=1) - onehot
    return (jnp.sum(before * onehot, axis=2), flat)


def dispatch_rows(normed, route_rows, blocks, slots_each, experts):
    block_len = normed.shape[0] // blocks
    positions, flat = slot_positions(route_rows, blocks, experts)
    block_index = jnp.arange(blocks, dtype=jnp.int32)[:, None]
    slot_index = block_index * slots_each + positions
    token_index = block_index * block_len + jnp.arange(2 * block_len, dtype=jnp.int32)[None, :] // 2
    table = jnp.full((blocks * slots_each, experts), -1, jnp.int32)
    table = table.at[slot_index.reshape(-1), flat.reshape(-1)].set(token_index.reshape(-1))
    fetched = normed[jnp.maximum(table, 0)]
    return jnp.where((table >= 0)[:, :, None], fetched, jnp.zeros_like(fetched))


def expert_half(
    expert_input,
    expert_gain,
    group_router,
    expert_router,
    routes,
    gate_weight,
    up_weight,
    down_weight,
):
    normed = norm_rows(expert_input, expert_gain)
    tp_count = lax.axis_size("tp")
    tp_place = lax.axis_index("tp")
    experts = expert_router.shape[1]
    block_len = normed.shape[0] // tp_count
    slots_each = 4 * block_len // experts
    own_rows = lax.dynamic_slice_in_dim(normed, tp_place * block_len, block_len, 0)
    own_routes = lax.dynamic_slice_in_dim(routes, tp_place * block_len, block_len, 0)
    sending = dispatch_rows(own_rows, own_routes, 1, slots_each, experts)
    arrived = lax.all_to_all(sending, "ep", split_axis=1, concat_axis=1, tiled=True)
    received = lax.all_gather(arrived, "tp", axis=0, tiled=True)
    held = gate_weight.shape[0]
    model = received.shape[2]
    down_whole = lax.all_gather(down_weight, "tp", axis=1, tiled=True)
    all_slots = received.reshape(received.shape[0], -1, held, model)
    gate = jnp.einsum("csed,edh->cseh", all_slots, gate_weight, preferred_element_type=jnp.float32)
    upward = jnp.einsum("csed,edh->cseh", all_slots, up_weight, preferred_element_type=jnp.float32)
    hidden = (jax.nn.silu(gate) * upward).astype(jnp.bfloat16)
    swapped = lax.all_to_all(hidden, "tp", split_axis=0, concat_axis=3, tiled=True)
    hid_part = hidden.shape[3]
    total = jnp.zeros((swapped.shape[0], swapped.shape[1], held, model), jnp.float32)
    for part in range(tp_count):
        partial_value = jnp.einsum(
            "cseh,ehd->csed",
            swapped[:, :, :, part * hid_part : (part + 1) * hid_part],
            down_whole[:, part * hid_part : (part + 1) * hid_part],
            preferred_element_type=jnp.float32,
        ).astype(jnp.bfloat16)
        partial_value = lax.optimization_barrier(partial_value)
        total = total + partial_value.astype(jnp.float32)
    summed = total.astype(jnp.bfloat16).reshape(slots_each, -1, model)
    returned = lax.all_to_all(summed, "ep", split_axis=1, concat_axis=1, tiled=True)
    positions, flat = slot_positions(own_routes, 1, experts)
    lookup = positions[0] * experts + flat[0]
    picked = (
        returned.reshape(slots_each * experts, model)[lookup]
        .astype(jnp.float32)
        .reshape(block_len, 2, model)
    )
    weights = route_weights(own_rows, group_router, expert_router, own_routes)
    return jnp.sum(picked * weights[:, :, None], axis=1).astype(jnp.bfloat16)


def on_device(
    mixer_input,
    mixer_gain,
    pool_in,
    pool_map,
    pool_scale,
    pool_out,
    expert_input,
    expert_gain,
    group_router,
    expert_router,
    routes,
    gate_weight,
    up_weight,
    down_weight,
):
    mixer_output = mixer_half(mixer_input, mixer_gain, pool_in, pool_map, pool_scale, pool_out)
    expert_output = expert_half(
        expert_input,
        expert_gain,
        group_router,
        expert_router,
        routes,
        gate_weight,
        up_weight,
        down_weight,
    )
    return (mixer_output, expert_output)


def solution(mesh):
    return jax.shard_map(
        on_device,
        mesh=mesh,
        in_specs=(
            P("ep", None),
            P(),
            P(None, "tp"),
            P("tp", None, None),
            P("tp"),
            P("tp", None),
            P("ep", None),
            P(),
            P(),
            P(),
            P("ep", None),
            P("ep", None, "tp"),
            P("ep", None, "tp"),
            P("ep", "tp", None),
        ),
        out_specs=(P(("ep", "tp"), None), P(("ep", "tp"), None)),
        check_vma=False,
    )
```

profile of v0, /device:TPU:8, one launch (start us, length us, event | category | flops | bytes accessed | tf_op | source)
XLA Modules:
  0.0 302.8 jit_solution(5306408200580199578)
XLA Ops:
  7.2 0.9 constant_dynamic-slice_fusion
  8.2 0.1 copy.41
  8.3 0.1 eq.66
  8.5 0.6 reduce-window.6
  9.1 0.2 slice_reduce_fusion
  9.4 0.1 reshape_reshape.3
  9.5 1.8 multiply_reduce_fusion
  11.3 2.0 convert_element_type.227
  13.5 0.1 broadcast.292
  13.7 0.1 fusion.52
  13.9 9.3 %scatter_fusion = s32[6,64]{1,0:T(8,128)S(1)} fusion(s32[6,64]{1,0:T(8,128)S(1)} %broadcast_in_dim.11, s32[192]{0:T(256)S(1)} %bitcast.129, s32[192]{0:T(256)S(1)} %and_select_fusion.1), kind=kCustom, calls=%fused_computation.2 | custom fusion | bytes 3840 | tf_op jit(solution)/shard_map/scatter | solution.py:91
  23.4 0.1 copy.46
  23.5 1.3 fusion.26
  24.8 2.5 gather_fusion
  27.2 1.0 copy_select_fusion
  28.2 63.1 %all_to_all.28 = bf16[6,64,2048]{2,0,1:T(8,128)(2,1)S(1)} all-to-all(bf16[6,64,2048]{2,0,1:T(8,128)(2,1)S(1)} %copy_select_fusion), channel_id=1, replica_groups=mesh['ep'=64,'tp'=4] {'ep'}, dimensions={1} | all-to-all | bytes 3145728 | tf_op jit(solution)/shard_map/all_to_all | solution.py:115
  91.4 2.0 copy.48
  93.5 0.7 all-gather.5.cloned.1.call-update
  94.2 0.8 copy-done.3
  95.0 0.5 fusion
  95.6 0.8 fusion.17
  96.4 0.7 copy-done.4
  97.1 1.9 collective-permute-start
  99.1 58.8 %all-gather.3.cloned.1.call-done = bf16[24,64,2048]{2,1,0:T(8,128)(2,1)} async-done(((bf16[6,64,2048]{2,1,0:T(8,128)(2,1)}), bf16[24,64,2048]{2,1,0:T(8,128)(2,1)}) %all-gather.3.cloned.1.call-update) | async-done | bytes 6291472 | tf_op jit(solution)/shard_map/all_gather | solution.py:116
  157.9 5.1 %fusion.23 = f32[24,64,256]{2,1,0:T(8,128)S(1)} fusion(bf16[24,64,2048]{2,1,0:T(8,128)(2,1)} %all-gather.3.cloned.1.call-done, bf16[1,2048,256]{2,1,0:T(8,128)(2,1)} %param.25), kind=kOutput, calls=%fused_computation.46 | convolution fusion | flops 1610612736 | bytes 8912896 | tf_op jit(solution)/shard_map/csed,edh->cseh/dot_general | solution.py:121
  163.1 3.0 fusion.16
  166.1 3.8 %all-to-all-start.1 = ((bf16[24,64,1,256]{3,1,2,0:T(8,128)(2,1)}), bf16[24,64,1,256]{3,1,2,0:T(8,128)(2,1)S(1)}, u32[]{:S(2)}, u32[]{:S(2)}) async-start(bf16[24,64,1,256]{3,1,2,0:T(8,128)(2,1)} %fusion.16), calls=%async_computation.2 | async-start | bytes 1572864 | tf_op jit(solution)/shard_map/all_to_all | solution.py:124
  170.0 3.3 %convolution_convert_fusion = bf16[512,2048]{1,0:T(8,128)(2,1)} fusion(bf16[256,2048]{1,0:T(8,128)(2,1)S(1)} %copy-done, f32[256]{0:T(256)S(1)} %convert_element_type.223, f32[527,256]{1,0:T(8,128)S(1)} %maximum_convert_fusion, f32[512]{0:T(512)S(1)} %minimum_convert_fusion, f32[]{:T(128)S(6)} %convert_element_type.220, f32[]{:T(128)S(6)} %convert_element_type.219, ...), kind=kOutput, calls=%fused_computation.10 | convolution fusion | flops 609746944 | bytes 11668544 | tf_op jit(solution)/shard_map/dot_general | solution.py:68
  173.4 14.8 %all-to-all-done.1 = bf16[24,64,1,256]{3,1,2,0:T(8,128)(2,1)S(1)} async-done(((bf16[24,64,1,256]{3,1,2,0:T(8,128)(2,1)}), bf16[24,64,1,256]{3,1,2,0:T(8,128)(2,1)S(1)}, u32[]{:S(2)}, u32[]{:S(2)}) %all-to-all-start.1) | async-done | bytes 786464 | tf_op jit(solution)/shard_map/all_to_all | solution.py:124
  188.2 0.6 copy.56
  188.8 0.6 all_to_all.23
  189.4 26.5 %all-gather.5.cloned.1.call-done = bf16[1,1024,2048]{2,1,0:T(8,128)(2,1)} async-done(((bf16[1,256,2048]{2,1,0:T(8,128)(2,1)}), bf16[1,1024,2048]{2,1,0:T(8,128)(2,1)}) %all-gather.5.cloned.1.call-update) | async-done | bytes 4194320 | tf_op jit(solution)/shard_map/all_gather | solution.py:119
  215.8 2.0 fusion.3
  217.8 1.8 fusion.4
  219.6 0.6 fusion.5
  220.2 0.6 fusion.6
  220.8 1.4 fusion.11
  222.2 2.2 copy.51
  224.4 10.9 %all-to-all-start.2 = ((bf16[6,64,2048]{2,0,1:T(8,128)(2,1)}), bf16[6,64,2048]{2,0,1:T(8,128)(2,1)}, u32[]{:S(2)}, u32[]{:S(2)}) async-start(bf16[6,64,2048]{2,0,1:T(8,128)(2,1)} %copy.51), calls=%async_computation.3 | async-start | bytes 4194304 | tf_op jit(solution)/shard_map/all_to_all | solution.py:137
  235.3 0.2 fusion.56
  235.6 0.3 convolution_exponential_fusion
  235.8 0.2 fusion.21
  236.1 0.2 convolution_multiply_fusion.1
  236.5 49.9 %all-to-all-done.2 = bf16[6,64,2048]{2,0,1:T(8,128)(2,1)} async-done(((bf16[6,64,2048]{2,0,1:T(8,128)(2,1)}), bf16[6,64,2048]{2,0,1:T(8,128)(2,1)}, u32[]{:S(2)}, u32[]{:S(2)}) %all-to-all-start.2) | async-done | bytes 1572896 | tf_op jit(solution)/shard_map/all_to_all | solution.py:137
  286.4 2.5 copy.52
  288.9 2.1 gather_fusion.1
  290.9 2.1 reshape.556
  293.1 3.1 %multiply_reduce_fusion.1 = bf16[96,2048]{1,0:T(8,128)(2,1)} fusion(f32[96,2,2048]{2,1,0:T(2,128)S(1)} %reshape.556, f32[96,2]{1,0:T(8,128)S(1)} %copy.53), kind=kLoop, calls=%fused_computation.31 | loop fusion | flops 589824 | bytes 1966848 | tf_op jit(solution)/shard_map/reduce_sum | solution.py:146
  (64 shorter events, 1.2 us)
Async XLA Ops:
  7.2 162.9 %copy-start = (bf16[256,2048]{1,0:T(8,128)(2,1)S(1)}, bf16[256,2048]{1,0:T(8,128)(2,1)}, u32[]{:S(2)}) copy-start(bf16[256,2048]{1,0:T(8,128)(2,1)} %param.19) | copy-start | bytes 3145732
  7.2 4.2 %copy-start.1 = (bf16[384,2048]{1,0:T(8,128)(2,1)S(1)}, bf16[384,2048]{1,0:T(8,128)(2,1)}, u32[]{:S(2)}) copy-start(bf16[384,2048]{1,0:T(8,128)(2,1)} %param.20) | copy-start | bytes 4718596
  7.2 150.7 %all-gather.3.cloned.1.call-start = ((), (), s32[]{:S(2)}) async-start(), calls=%async_computation.5 | async-start | bytes 7864320 | tf_op jit(solution)/shard_map/all_gather | solution.py:116
  13.4 10.0 %copy-start.8 = (bf16[2048]{0:T(1024)(128)(2,1)S(1)}, bf16[2048]{0:T(1024)(128)(2,1)}, u32[]{:S(2)}) copy-start(bf16[2048]{0:T(1024)(128)(2,1)} %param.21) | copy-start | bytes 12292
  93.4 0.8 copy-start.9
  93.4 1.6 copy-start.3
  93.4 122.4 %all-gather.5.cloned.1.call-start = ((), (), s32[]{:S(2)}) async-start(), calls=%async_computation.6 | async-start | bytes 5242880 | tf_op jit(solution)/shard_map/all_gather | solution.py:119
  94.2 1.4 copy-start.11
  95.6 3.5 %copy-start.14 = (bf16[256]{0:T(256)(128)(2,1)S(1)}, bf16[256]{0:T(256)(128)(2,1)}, u32[]{:S(2)}) copy-start(bf16[256]{0:T(256)(128)(2,1)} %param.18) | copy-start | bytes 1540
  96.4 0.7 copy-start.4
  97.1 72.9 %collective-permute-start = (bf16[15,256]{1,0:T(8,128)(2,1)S(1)}, bf16[15,256]{1,0:T(8,128)(2,1)S(1)}, u32[]{:S(2)}, u32[]{:S(2)}) collective-permute-start(bf16[15,256]{1,0:T(8,128)(2,1)S(1)} %slice.135), channel_id=1, source_target_pairs={{0,4},{4,8},{8,12},{12,16},{16,20},{20,24},{24,28},{28,32},{32,36}... | collective-permute-start | bytes 23048 | tf_op jit(solution)/shard_map/ppermute | solution.py:13
  157.9 5.1 %copy-start.10 = (bf16[24,64,2048]{2,1,0:T(8,128)(2,1)S(1)}, bf16[24,64,2048]{2,1,0:T(8,128)(2,1)}, u32[]{:S(2)}) copy-start(bf16[24,64,2048]{2,1,0:T(8,128)(2,1)} %all-gather.3.cloned.1.call-done) | copy-start | bytes 18874372
  157.9 5.1 %copy-start.12 = (bf16[1,2048,256]{2,1,0:T(8,128)(2,1)S(1)}, bf16[1,2048,256]{2,1,0:T(8,128)(2,1)}, u32[]{:S(2)}) copy-start(bf16[1,2048,256]{2,1,0:T(8,128)(2,1)} %param.26) | copy-start | bytes 3145732
  163.1 6.9 %copy-start.5 = (bf16[512,256]{1,0:T(8,128)(2,1)S(1)}, bf16[512,256]{1,0:T(8,128)(2,1)}, u32[]{:S(2)}) copy-start(bf16[512,256]{1,0:T(8,128)(2,1)} %copy-done.4) | copy-start | bytes 786436
  166.1 4.0 %copy-start.13 = (bf16[1,256,256]{2,1,0:T(8,128)(2,1)S(1)}, bf16[1,256,256]{2,1,0:T(8,128)(2,1)}, u32[]{:S(2)}) copy-start(bf16[1,256,256]{2,1,0:T(8,128)(2,1)} %param.17) | copy-start | bytes 393220
  166.1 22.1 %all-to-all-start.1 = ((bf16[24,64,1,256]{3,1,2,0:T(8,128)(2,1)}), bf16[24,64,1,256]{3,1,2,0:T(8,128)(2,1)S(1)}, u32[]{:S(2)}, u32[]{:S(2)}) async-start(bf16[24,64,1,256]{3,1,2,0:T(8,128)(2,1)} %fusion.16), calls=%async_computation.2 | async-start | bytes 1572864 | tf_op jit(solution)/shard_map/all_to_all | solution.py:124
  169.9 126.4 %reduce-scatter.2.cloned.1.call-start = ((), (), s32[]{:S(2)}) async-start(), calls=%async_computation.4 | async-start | bytes 2621440 | tf_op jit(solution)/shard_map/reduce_scatter | solution.py:67
  215.8 3.8 %copy-start.2 = (bf16[1,1024,2048]{2,1,0:T(8,128)(2,1)S(1)}, bf16[1,1024,2048]{2,1,0:T(8,128)(2,1)}, u32[]{:S(2)}) copy-start(bf16[1,1024,2048]{2,1,0:T(8,128)(2,1)} %all-gather.5.cloned.1.call-done) | copy-start | bytes 12582916
  224.4 10.9 %copy-start.7 = (bf16[2048,4]{0,1:T(4,128)(2,1)S(1)}, bf16[2048,4]{0,1:T(4,128)(2,1)}, u32[]{:S(2)}) copy-start(bf16[2048,4]{0,1:T(4,128)(2,1)} %param.22) | copy-start | bytes 49156
  224.4 11.2 %copy-start.6 = (bf16[2048,64]{0,1:T(8,128)(2,1)S(1)}, bf16[2048,64]{0,1:T(8,128)(2,1)}, u32[]{:S(2)}) copy-start(bf16[2048,64]{0,1:T(8,128)(2,1)} %param.23) | copy-start | bytes 786436
  224.4 62.0 %all-to-all-start.2 = ((bf16[6,64,2048]{2,0,1:T(8,128)(2,1)}), bf16[6,64,2048]{2,0,1:T(8,128)(2,1)}, u32[]{:S(2)}, u32[]{:S(2)}) async-start(bf16[6,64,2048]{2,0,1:T(8,128)(2,1)} %copy.51), calls=%async_computation.3 | async-start | bytes 4194304 | tf_op jit(solution)/shard_map/all_to_all | solution.py:137
Sparse Core Ops, SparseCore 0:
  93.5 64.3 all-gather.2
  159.7 56.0 all-gather.4
  219.0 31.9 reduce-scatter.1
where the time goes:
time: 303 us
  waiting for transfers between devices  151 us (50%)
  blocking collectives  63.1 us (21%)
  local copies, waits for them, and re-layouts  27.7 us (9%)
  matrix products  18 us (6%)
  starting transfers between devices  16.7 us (6%)
  between operations  14.2 us (5%)
  other arithmetic  12.1 us (4%)
    all_to_all x1, blocking collectives, expert_half(): lax.all_to_all(sending, 'ep', split_axis=1, concat_axis=1, tiled=True)  63.1 us
    all_gather x1, waiting for transfers between devices, expert_half(): received = lax.all_gather(arrived, 'tp', axis=0, tiled=True)  58.8 us
    all_to_all x1, waiting for transfers between devices, expert_half(): lax.all_to_all(summed, 'ep', split_axis=1, concat_axis=1, tiled=True)  49.9 us
    all_gather x1, waiting for transfers between devices, expert_half(): down_whole = lax.all_gather(down_weight, 'tp', axis=1, tiled=True)  26.5 us
    all_to_all x1, waiting for transfers between devices, expert_half(): lax.all_to_all(hidden, 'tp', split_axis=0, concat_axis=3, tiled=True)  14.8 us
    all_to_all x1, starting transfers between devices, expert_half(): lax.all_to_all(summed, 'ep', split_axis=1, concat_axis=1, tiled=True)  10.9 us
    scatter x1, local copies, waits for them, and re-layouts, dispatch_rows(): table.at[slot_index.reshape(-1), flat.reshape(-1)]  9.28 us
  transfers between devices with their start and end apart: 6, of which 4 were waited for; matrix products, arithmetic and copies ran while one was open for 11% of the time, Pallas kernels for 0%

commit v1 on v0

--- a/solution.py
+++ b/solution.py
@@ -5,6 +5,28 @@
 
 RIM = 15
 EPS = 1e-06
+
+
+def joined_along(parts, dim):
+    parts = jnp.moveaxis(parts, 0, dim)
+    lengths = parts.shape
+    return parts.reshape(*lengths[:dim], lengths[dim] * lengths[dim + 1], *lengths[dim + 2 :])
+
+
+def ring_gather(x, axis, dim):
+    size = lax.axis_size(axis)
+    pairs = [(i, (i + 1) % size) for i in range(size)]
+    back = [(b, a) for a, b in pairs]
+    lower, upper = ([], [])
+    for step in range(size - 1):
+        if step % 2 == 0:
+            lower.append(lax.ppermute(lower[-1] if lower else x, axis, pairs))
+        else:
+            upper.append(lax.ppermute(upper[-1] if upper else x, axis, back))
+    parts = jnp.stack([*lower[::-1], x, *upper])
+    shift = lax.axis_index(axis) - len(lower)
+    parts = parts[(jnp.arange(size) - shift) % size]
+    return joined_along(parts, dim)
 
 
 def passed_along(value, axis, steps):
@@ -116,7 +138,7 @@
     received = lax.all_gather(arrived, "tp", axis=0, tiled=True)
     held = gate_weight.shape[0]
     model = received.shape[2]
-    down_whole = lax.all_gather(down_weight, "tp", axis=1, tiled=True)
+    down_whole = ring_gather(down_weight, "tp", 1)
     all_slots = received.reshape(received.shape[0], -1, held, model)
     gate = jnp.einsum("csed,edh->cseh", all_slots, gate_weight, preferred_element_type=jnp.float32)
     upward = jnp.einsum("csed,edh->cseh", all_slots, up_weight, preferred_element_type=jnp.float32)

time: 303 us -> 303 us (level)
  waiting for transfers between devices: 151 us -> 138 us
  local copies, waits for them, and re-layouts: 27.7 us -> 32.8 us
  other arithmetic: 12.1 us -> 16.6 us
    ppermute x0 -> x3, waiting for transfers between devices: none -> 28.8 us  [the longest x2 28.8 us: ring_gather(): lower.append(lax.ppermute(lower[-1] if lower else x, axis, pairs))]
    all_gather x1 -> x0, waiting for transfers between devices: 26.5 us -> none  [expert_half(): down_whole = lax.all_gather(down_weight, 'tp', axis=1, tiled=True)]
    all_to_all x1, waiting for transfers between devices: 14.8 us -> 0.01 us  [expert_half(): lax.all_to_all(hidden, 'tp', split_axis=0, concat_axis=3, tiled=True)]
    gather x0 -> x1, local copies, waits for them, and re-layouts: none -> 4.97 us  [ring_gather(): parts = parts[(jnp.arange(size) - shift) % size]]
    ppermute x0 -> x3, starting transfers between devices: none -> 4.94 us  [the longest x2 3.2 us: ring_gather(): lower.append(lax.ppermute(lower[-1] if lower else x, axis, pairs))]
    all_to_all x1, starting transfers between devices: 10.9 us -> 7.18 us  [expert_half(): lax.all_to_all(summed, 'ep', split_axis=1, concat_axis=1, tiled=True)]
    another operation x3 -> x4, other arithmetic: 0.72 us -> 4.29 us  [the longest x1 3.58 us: ring_gather(): parts = jnp.stack([*lower[::-1], x, *upper])]
  transfers between devices with their start and end apart: 6 -> 8, of which waited for: 4 -> 4; matrix products, arithmetic and copies ran while one was open for 11% -> 14% of each run, Pallas kernels for 0% -> 0%
where the time goes in v1:
time: 303 us; the launch traced here: 302 us
  waiting for transfers between devices  138 us (46%)
  blocking collectives  63.1 us (21%)
  local copies, waits for them, and re-layouts  32.8 us (11%)
  matrix products  19.2 us (6%)
  starting transfers between devices  17.6 us (6%)
  other arithmetic  16.6 us (5%)
  between operations  14.6 us (5%)
    all_to_all x1, blocking collectives, expert_half(): lax.all_to_all(sending, 'ep', split_axis=1, concat_axis=1, tiled=True)  63.1 us
    all_gather x1, waiting for transfers between devices, expert_half(): received = lax.all_gather(arrived, 'tp', axis=0, tiled=True)  56.5 us
    all_to_all x1, waiting for transfers between devices, expert_half(): lax.all_to_all(summed, 'ep', split_axis=1, concat_axis=1, tiled=True)  50 us
    ppermute x2, waiting for transfers between devices, ring_gather(): lower.append(lax.ppermute(lower[-1] if lower else x, axis, pairs))  28.8 us
    scatter x1, local copies, waits for them, and re-layouts, dispatch_rows(): table.at[slot_index.reshape(-1), flat.reshape(-1)]  9.28 us
    all_to_all x1, starting transfers between devices, expert_half(): lax.all_to_all(summed, 'ep', split_axis=1, concat_axis=1, tiled=True)  7.18 us
  transfers between devices with their start and end apart: 8, of which 4 were waited for; matrix products, arithmetic and copies ran while one was open for 14% of the time, Pallas kernels for 0%

profile of v1, /device:TPU:8, one launch (start us, length us, event | category | flops | bytes accessed | tf_op | source)
XLA Modules:
  0.0 302.2 jit_solution(9516516437188427487)
XLA Ops:
  7.2 0.9 constant_dynamic-slice_fusion
  8.5 0.6 reduce-window.6
  9.1 0.2 slice_reduce_fusion
  9.4 0.1 reshape_reshape.3
  9.5 1.8 multiply_reduce_fusion
  11.3 2.0 convert_element_type.215
  13.9 9.3 %scatter_fusion = s32[6,64]{1,0:T(8,128)S(1)} fusion(s32[6,64]{1,0:T(8,128)S(1)} %broadcast_in_dim.11, s32[192]{0:T(256)S(1)} %bitcast.130, s32[192]{0:T(256)S(1)} %and_select_fusion.1), kind=kCustom, calls=%fused_computation.3 | custom fusion | bytes 3840 | tf_op jit(solution)/shard_map/scatter | solution.py:113
  23.5 1.3 fusion.26
  24.8 2.5 gather_fusion.1
  27.2 1.0 copy_select_fusion
  28.2 63.1 %all_to_all.28 = bf16[6,64,2048]{2,0,1:T(8,128)(2,1)S(1)} all-to-all(bf16[6,64,2048]{2,0,1:T(8,128)(2,1)S(1)} %copy_select_fusion), channel_id=1, replica_groups=mesh['ep'=64,'tp'=4] {'ep'}, dimensions={1} | all-to-all | bytes 3145728 | tf_op jit(solution)/shard_map/all_to_all | solution.py:137
  91.4 2.0 copy.48
  93.4 1.6 collective-permute-start.1
  95.0 1.7 collective-permute-start.3
  96.7 0.5 fusion
  97.3 0.8 fusion.17
  98.0 0.7 copy-done.5
  98.7 1.9 collective-permute-start
  100.8 2.9 collective-permute-done
  103.7 1.0 maximum_convert_fusion
  104.7 28.8 %collective-permute-done.1 = bf16[1,256,2048]{2,1,0:T(8,128)(2,1)} collective-permute-done((bf16[1,256,2048]{2,1,0:T(8,128)(2,1)}, bf16[1,256,2048]{2,1,0:T(8,128)(2,1)}, u32[]{:S(2)}, u32[]{:S(2)}) %collective-permute-start.1) | collective-permute-done | bytes 1048608 | tf_op jit(solution)/shard_map/ppermute | solution.py:23
  133.5 1.6 collective-permute-start.2
  135.2 56.5 %all-gather.2.cloned.1.call-done = bf16[24,64,2048]{2,1,0:T(8,128)(2,1)} async-done(((bf16[6,64,2048]{2,1,0:T(8,128)(2,1)}), bf16[24,64,2048]{2,1,0:T(8,128)(2,1)}) %all-gather.2.cloned.1.call-update) | async-done | bytes 6291472 | tf_op jit(solution)/shard_map/all_gather | solution.py:138
  191.7 5.1 %fusion.23 = f32[24,64,256]{2,1,0:T(8,128)S(1)} fusion(bf16[24,64,2048]{2,1,0:T(8,128)(2,1)} %all-gather.2.cloned.1.call-done, bf16[1,2048,256]{2,1,0:T(8,128)(2,1)} %param.25), kind=kOutput, calls=%fused_computation.48 | convolution fusion | flops 1610612736 | bytes 8912896 | tf_op jit(solution)/shard_map/csed,edh->cseh/dot_general | solution.py:143
  196.8 4.2 %fusion.16 = bf16[24,64,1,256]{3,1,2,0:T(8,128)(2,1)} fusion(bf16[24,64,2048]{2,1,0:T(8,128)(2,1)S(1)} %copy-done.10, f32[24,64,256]{2,1,0:T(8,128)S(1)} %fusion.23, bf16[1,2048,256]{2,1,0:T(8,128)(2,1)} %param.26), kind=kOutput, calls=%fused_computation.34 | convolution fusion | flops 1612972032 | bytes 9699328 | tf_op jit(solution)/shard_map/csed,edh->cseh/dot_general | solution.py:144
  201.0 3.5 %all-to-all-start.1 = ((bf16[24,64,1,256]{3,1,2,0:T(8,128)(2,1)}), bf16[24,64,1,256]{3,1,2,0:T(8,128)(2,1)S(1)}, u32[]{:S(2)}, u32[]{:S(2)}) async-start(bf16[24,64,1,256]{3,1,2,0:T(8,128)(2,1)} %fusion.16), calls=%async_computation.2 | async-start | bytes 1572864 | tf_op jit(solution)/shard_map/all_to_all | solution.py:146
  204.6 3.2 %convolution_convert_fusion = bf16[512,2048]{1,0:T(8,128)(2,1)} fusion(bf16[256,2048]{1,0:T(8,128)(2,1)S(1)} %copy-done, f32[256]{0:T(256)S(1)} %convert_element_type.211, f32[527,256]{1,0:T(8,128)S(1)} %maximum_convert_fusion, f32[512]{0:T(512)S(1)} %minimum_convert_fusion, f32[]{:T(128)S(6)} %convert_element_type.208, f32[]{:T(128)S(6)} %convert_element_type.207, ...), kind=kOutput, calls=%fused_computation.12 | convolution fusion | flops 609746944 | bytes 11668544 | tf_op jit(solution)/shard_map/dot_general | solution.py:90
  207.9 1.2 copy-done.4
  209.0 3.6 %maximum_bitcast_fusion = bf16[4,256,2048]{2,1,0:T(8,128)(2,1)} fusion(bf16[1,1,256,2048]{3,2,1,0:T(8,128)(2,1)} %bitcast.4, bf16[1,1,256,2048]{3,2,1,0:T(8,128)(2,1)S(1)} %bitcast.138, bf16[1,1,256,2048]{3,2,1,0:T(8,128)(2,1)} %bitcast.2, bf16[1,1,256,2048]{3,2,1,0:T(8,128)(2,1)} %bitcast.1), kind=kLoop, calls=%fused_computation.9 | loop fusion | flops 6291456 | bytes 8388608 | tf_op jit(solution)/shard_map/stack | solution.py:26
  212.6 5.0 %gather_fusion = bf16[4,256,2048]{2,1,0:T(8,128)(2,1)} fusion(bf16[4,256,2048]{2,1,0:T(8,128)(2,1)} %maximum_bitcast_fusion, s32[1024]{0:T(1024)S(1)} %pad_clamp_fusion.2), kind=kCustom, calls=%fused_computation | custom fusion | bytes 8388624 | tf_op jit(solution)/shard_map/gather | solution.py:28
  217.6 0.6 copy.56
  218.2 0.6 all_to_all.23
  218.8 2.0 fusion.3
  220.7 1.8 fusion.4
  222.6 0.6 fusion.5
  223.1 0.6 fusion.6
  223.7 1.4 fusion.11
  225.1 2.2 copy.51
  227.3 7.2 %all-to-all-start.2 = ((bf16[6,64,2048]{2,0,1:T(8,128)(2,1)}), bf16[6,64,2048]{2,0,1:T(8,128)(2,1)}, u32[]{:S(2)}, u32[]{:S(2)}) async-start(bf16[6,64,2048]{2,0,1:T(8,128)(2,1)} %copy.51), calls=%async_computation.3 | async-start | bytes 4194304 | tf_op jit(solution)/shard_map/all_to_all | solution.py:159
  234.5 0.2 fusion.58
  234.7 0.3 convolution_exponential_fusion
  235.0 0.2 fusion.21
  235.2 0.2 convolution_multiply_fusion.1
  235.7 50.0 %all-to-all-done.2 = bf16[6,64,2048]{2,0,1:T(8,128)(2,1)} async-done(((bf16[6,64,2048]{2,0,1:T(8,128)(2,1)}), bf16[6,64,2048]{2,0,1:T(8,128)(2,1)}, u32[]{:S(2)}, u32[]{:S(2)}) %all-to-all-start.2) | async-done | bytes 1572896 | tf_op jit(solution)/shard_map/all_to_all | solution.py:159
  285.6 2.5 copy.52
  288.1 2.0 gather_fusion.2
  290.1 2.1 reshape.605
  292.3 3.1 %multiply_reduce_fusion.1 = bf16[96,2048]{1,0:T(8,128)(2,1)} fusion(f32[96,2,2048]{2,1,0:T(2,128)S(1)} %reshape.605, f32[96,2]{1,0:T(8,128)S(1)} %copy.53), kind=kLoop, calls=%fused_computation.33 | loop fusion | flops 589824 | bytes 1966848 | tf_op jit(solution)/shard_map/reduce_sum | solution.py:168
  (69 shorter events, 1.6 us)
Async XLA Ops:
  7.2 197.4 %copy-start = (bf16[256,2048]{1,0:T(8,128)(2,1)S(1)}, bf16[256,2048]{1,0:T(8,128)(2,1)}, u32[]{:S(2)}) copy-start(bf16[256,2048]{1,0:T(8,128)(2,1)} %param.19) | copy-start | bytes 3145732
  7.2 4.2 %copy-start.1 = (bf16[384,2048]{1,0:T(8,128)(2,1)S(1)}, bf16[384,2048]{1,0:T(8,128)(2,1)}, u32[]{:S(2)}) copy-start(bf16[384,2048]{1,0:T(8,128)(2,1)} %param.20) | copy-start | bytes 4718596
  7.2 184.5 %all-gather.2.cloned.1.call-start = ((), (), s32[]{:S(2)}) async-start(), calls=%async_computation.5 | async-start | bytes 7864320 | tf_op jit(solution)/shard_map/all_gather | solution.py:138
  13.4 10.0 %copy-start.8 = (bf16[2048]{0:T(1024)(128)(2,1)S(1)}, bf16[2048]{0:T(1024)(128)(2,1)}, u32[]{:S(2)}) copy-start(bf16[2048]{0:T(1024)(128)(2,1)} %param.21) | copy-start | bytes 12292
  91.4 5.4 %copy-start.3 = (bf16[512,2048]{1,0:T(8,128)(2,1)S(1)}, bf16[512,2048]{1,0:T(8,128)(2,1)}, u32[]{:S(2)}) copy-start(bf16[512,2048]{1,0:T(8,128)(2,1)} %param.14) | copy-start | bytes 6291460
  93.4 3.8 %copy-start.9 = (bf16[2048]{0:T(1024)(128)(2,1)S(1)}, bf16[2048]{0:T(1024)(128)(2,1)}, u32[]{:S(2)}) copy-start(bf16[2048]{0:T(1024)(128)(2,1)} %param.15) | copy-start | bytes 12292
  93.4 3.8 %copy-start.11 = (bf16[2048,256]{1,0:T(8,128)(2,1)S(1)}, bf16[2048,256]{1,0:T(8,128)(2,1)}, u32[]{:S(2)}) copy-start(bf16[2048,256]{1,0:T(8,128)(2,1)} %param.16) | copy-start | bytes 3145732
  93.4 40.1 %collective-permute-start.1 = (bf16[1,256,2048]{2,1,0:T(8,128)(2,1)}, bf16[1,256,2048]{2,1,0:T(8,128)(2,1)}, u32[]{:S(2)}, u32[]{:S(2)}) collective-permute-start(bf16[1,256,2048]{2,1,0:T(8,128)(2,1)} %param.27), channel_id=1, source_target_pairs={{0,1},{1,2},{2,3},{3,0},{4,5},{5,6},{6,7},{7,4},{8,9},{9,10},{10,1... | collective-permute-start | bytes 3145736 | tf_op jit(solution)/shard_map/ppermute | solution.py:23
  95.0 112.9 %collective-permute-start.3 = (bf16[1,256,2048]{2,1,0:T(8,128)(2,1)}, bf16[1,256,2048]{2,1,0:T(8,128)(2,1)}, u32[]{:S(2)}, u32[]{:S(2)}) collective-permute-start(bf16[1,256,2048]{2,1,0:T(8,128)(2,1)} %param.27), channel_id=1, source_target_pairs={{1,0},{2,1},{3,2},{0,3},{5,4},{6,5},{7,6},{4,7},{9,8},{10,9},{11,1... | collective-permute-start | bytes 3145736 | tf_op jit(solution)/shard_map/ppermute | solution.py:25
  97.2 3.5 %copy-start.13 = (bf16[256]{0:T(256)(128)(2,1)S(1)}, bf16[256]{0:T(256)(128)(2,1)}, u32[]{:S(2)}) copy-start(bf16[256]{0:T(256)(128)(2,1)} %param.18) | copy-start | bytes 1540
  98.0 0.7 copy-start.5
  98.7 5.0 %collective-permute-start = (bf16[15,256]{1,0:T(8,128)(2,1)S(1)}, bf16[15,256]{1,0:T(8,128)(2,1)S(1)}, u32[]{:S(2)}, u32[]{:S(2)}) collective-permute-start(bf16[15,256]{1,0:T(8,128)(2,1)S(1)} %slice.137), channel_id=1, source_target_pairs={{0,4},{4,8},{8,12},{12,16},{16,20},{20,24},{24,28},{28,32},{32,36}... | collective-permute-start | bytes 23048 | tf_op jit(solution)/shard_map/ppermute | solution.py:35
  133.5 74.3 %collective-permute-start.2 = (bf16[1,256,2048]{2,1,0:T(8,128)(2,1)}, bf16[1,256,2048]{2,1,0:T(8,128)(2,1)}, u32[]{:S(2)}, u32[]{:S(2)}) collective-permute-start(bf16[1,256,2048]{2,1,0:T(8,128)(2,1)} %collective-permute-done.1), channel_id=1, source_target_pairs={{0,1},{1,2},{2,3},{3,0},{4,5},{5,6},{6,7},{7,4},{8,9},{9,10},{10,1... | collective-permute-start | bytes 3145736 | tf_op jit(solution)/shard_map/ppermute | solution.py:23
  191.7 5.1 %copy-start.10 = (bf16[24,64,2048]{2,1,0:T(8,128)(2,1)S(1)}, bf16[24,64,2048]{2,1,0:T(8,128)(2,1)}, u32[]{:S(2)}) copy-start(bf16[24,64,2048]{2,1,0:T(8,128)(2,1)} %all-gather.2.cloned.1.call-done) | copy-start | bytes 18874372
  196.8 7.8 %copy-start.12 = (bf16[1,256,256]{2,1,0:T(8,128)(2,1)S(1)}, bf16[1,256,256]{2,1,0:T(8,128)(2,1)}, u32[]{:S(2)}) copy-start(bf16[1,256,256]{2,1,0:T(8,128)(2,1)} %param.17) | copy-start | bytes 393220
  201.0 16.6 %all-to-all-start.1 = ((bf16[24,64,1,256]{3,1,2,0:T(8,128)(2,1)}), bf16[24,64,1,256]{3,1,2,0:T(8,128)(2,1)S(1)}, u32[]{:S(2)}, u32[]{:S(2)}) async-start(bf16[24,64,1,256]{3,1,2,0:T(8,128)(2,1)} %fusion.16), calls=%async_computation.2 | async-start | bytes 1572864 | tf_op jit(solution)/shard_map/all_to_all | solution.py:146
  204.5 90.8 %reduce-scatter.2.cloned.1.call-start = ((), (), s32[]{:S(2)}) async-start(), calls=%async_computation.4 | async-start | bytes 2621440 | tf_op jit(solution)/shard_map/reduce_scatter | solution.py:89
  207.8 1.2 copy-start.4
  218.8 3.8 %copy-start.2 = (bf16[4,256,2048]{2,1,0:T(8,128)(2,1)S(1)}, bf16[4,256,2048]{2,1,0:T(8,128)(2,1)}, u32[]{:S(2)}) copy-start(bf16[4,256,2048]{2,1,0:T(8,128)(2,1)} %gather_fusion) | copy-start | bytes 12582916
  227.3 7.2 %copy-start.7 = (bf16[2048,4]{0,1:T(4,128)(2,1)S(1)}, bf16[2048,4]{0,1:T(4,128)(2,1)}, u32[]{:S(2)}) copy-start(bf16[2048,4]{0,1:T(4,128)(2,1)} %param.22) | copy-start | bytes 49156
  227.3 7.4 %copy-start.6 = (bf16[2048,64]{0,1:T(8,128)(2,1)S(1)}, bf16[2048,64]{0,1:T(8,128)(2,1)}, u32[]{:S(2)}) copy-start(bf16[2048,64]{0,1:T(8,128)(2,1)} %param.23) | copy-start | bytes 786436
  227.3 58.3 %all-to-all-start.2 = ((bf16[6,64,2048]{2,0,1:T(8,128)(2,1)}), bf16[6,64,2048]{2,0,1:T(8,128)(2,1)}, u32[]{:S(2)}, u32[]{:S(2)}) async-start(bf16[6,64,2048]{2,0,1:T(8,128)(2,1)} %copy.51), calls=%async_computation.3 | async-start | bytes 4194304 | tf_op jit(solution)/shard_map/all_to_all | solution.py:159
Sparse Core Ops, SparseCore 0:
  93.5 98.1 all-gather.1
  208.4 30.2 reduce-scatter.1
